TPU v7x, 256 devices: a whole 4x4x8 slice. The times are simulated.
256 devices in a mesh: sp: 32 (over z, y), tp: 8 (over x, core).
Axes of the slice: x: 4, y: 4, z: 8, core: 2. Of those that a mesh axis runs over, the one named last changes fastest.
Arguments:
- inputs: bfloat16 [16384, 4096], P('sp', 'tp'), may hold values from -24 to 24
- length: int32 [1], replicated, may hold values from 8193 to 16384
- win_query: bfloat16 [4096, 1536], P(None, 'tp'), may hold values from -8 to 8
- win_key: bfloat16 [4096, 512], P(None, 'tp'), may hold values from -8 to 8
- win_value: bfloat16 [4096, 512], P(None, 'tp'), may hold values from -1.5 to 1.5
- sink_logit: float32 [24], P('tp'), may hold values from 4 to 8
- diff_query: bfloat16 [4096, 1024], P(None, 'tp'), may hold values from -8 to 8
- diff_key: bfloat16 [4096, 1024], P(None, 'tp'), may hold values from -8 to 8
- diff_value: bfloat16 [4096, 1024], P(None, 'tp'), may hold values from -0.09375 to 0.09375
- mix_lambda: float32 [16], P('tp'), may hold values from 0.3 to 0.8
- head_gain: float32 [64], replicated, may hold values from 0.1 to 1.9
- win_out: bfloat16 [1536, 4096], P('tp'), may hold values from -0.125 to 0.125
- diff_out: bfloat16 [1024, 4096], P('tp'), may hold values from -0.125 to 0.125
Outputs:
- merged_out: bfloat16 [16384, 4096], P(('sp', 'tp'))
All inputs are finite; a program needn't handle non-finite values.
Results may differ from a plain program's by a relative error of at most 0.015.
Values may be sent and summed in bfloat16 or wider, within the bound.
A program may use at most 128 MiB of HBM per device.

v0:
```python
import functools

import jax
import jax.numpy as jnp
from jax import lax
from jax.experimental import pallas as pl
from jax.experimental.pallas import tpu as pltpu
from jax.sharding import PartitionSpec as P

HEAD = 64
DQK = 32
GROUP = 3
WINDOW = 128
NX, NY, NZ = 4, 4, 8
ROWS = 512
QUARTER = ROWS // 4
HALF = ROWS // 2
BLOCKS = NY * NZ
Q_SCALE = 1.4426950408889634 * DQK ** (-0.5)
MESH = pl.DeviceIdType.MESH

epsilon = 1e-06
masked_score = -1e30
VMEM_SPEC = pl.BlockSpec(memory_space=pltpu.VMEM)
SMEM_SPEC = pl.BlockSpec(memory_space=pltpu.SMEM)
HBM_SPEC = pl.BlockSpec(memory_space=pltpu.HBM)


def place():
    sp, tp = lax.axis_index("sp"), lax.axis_index("tp")
    return sp // NY, sp % NY, tp // 2, tp % 2


def greet(devices, conditions=None):
    barrier = pltpu.get_barrier_semaphore()
    for i, device in enumerate(devices):
        def signal(device=device):
            pl.semaphore_signal(barrier, inc=1, device_id=device, device_id_type=MESH)
        if conditions is None or conditions[i] is None:
            signal()
        else:
            pl.when(conditions[i])(signal)


WQ, DQ, DK, DV, ACC_COLS = 0, 384, 512, 640, 768
TILE = 2 * ROWS
CHUNK = 1024
CHUNKS = 4
SHARE = 32
GROUPS = 2 * NX


def natural(r, u):
    return (r // SHARE) * 2 * SHARE + u * SHARE + r % SHARE


def layer_kernel(
    length_ref, lam_smem, sink_ref, x_ref, gain_ref, wq_hbm, wk_hbm, wv_hbm, dq_hbm, dk_hbm, dv_hbm, wo_hbm, do_hbm,
    out_ref,
    xg, wt, dq, dk, dv, wo, do, acc, msg, lam_ref, lamo_ref, halo_ref, winq, keys, v_t, win_ref,
    kv_ref, q_ref, qz, va, att, s_buf, t_buf, m_buf, bias,
    o_buf, rows_t, diff_rows, lhs_w, lhs_d, give, take, mine, far_in, joined, fin,
    w_sem, recv_x, send_xr, send_xl, send_xs,
    recv_kv, recv_q, recv_lam, recv_halo, send_a, send_lam, send_ring, send_sib, send_halo, local_sem,
    recv_o, send_o, send_g, recv_g, send_f, recv_f, send_n, recv_n,
):
    z, y, x, c = place()
    sp = z * NY + y
    tp = x * 2 + c
    live = length_ref[0]
    right = (sp, ((x + 1) % NX) * 2 + c)
    left = (sp, ((x + NX - 1) % NX) * 2 + c)
    sibling = (sp, x * 2 + 1 - c)
    up = (((z + 1) % NZ) * NY + y, tp)
    down = (((z + NZ - 1) % NZ) * NY + y, tp)
    after = ((sp + 1) % BLOCKS, tp)
    before = ((sp + BLOCKS - 1) % BLOCKS, tp)
    partners = [(z * NY + 2 * c + i, x * 2 + y // 2) for i in range(2)]
    away = [(2 * c + i) != y for i in range(2)]

    loads = [
        pltpu.make_async_copy(src, dst, w_sem.at[i])
        for i, (src, dst) in enumerate(
            (
                (wq_hbm, wt.at[pl.ds(0, 192)]),
                (wk_hbm, wt.at[pl.ds(192, 64)]),
                (wv_hbm, wt.at[pl.ds(256, 64)]),
                (dq_hbm, dq),
                (dk_hbm, dk),
                (dv_hbm, dv),
                (wo_hbm, wo),
                (do_hbm, do),
            )
        )
    ]
    for load in loads:
        load.start()
    for i in range(2):
        lam_ref[i] = jnp.full((8, 128), lam_smem[i], jnp.float32)
    greet(
        (right, left, sibling, up, down, after, before) + tuple(partners), (None,) * 7 + tuple(away)
    )
    pl.semaphore_wait(pltpu.get_barrier_semaphore(), 7 + sum(a.astype(jnp.int32) for a in away))

    started = []

    def remote(src, dst, send_sem, recv_sem, device):
        return pltpu.make_async_remote_copy(
            src_ref=src, dst_ref=dst, send_sem=send_sem, recv_sem=recv_sem,
            device_id=device, device_id_type=MESH,
        )

    def go(copy):
        copy.start()
        started.append(copy)

    def send_x(own, t, q, device, sem):
        part = pl.ds(q % 2 * 4, 4)
        src = x_ref.at[part, q // 2] if own else xg.at[t, q // 2, part]
        go(remote(src, xg.at[t, q // 2, part], sem, recv_x.at[t, q], device))

    def arrive_x(t, q):
        part = xg.at[t, q // 2, pl.ds(q % 2 * 4, 4)]
        remote(part, part, send_xr.at[0], recv_x.at[t, q], sibling).wait_recv()

    t_left = ((x + NX - 1) % NX) * 2 + c
    t_right = ((x + 1) % NX) * 2 + c
    t_far = ((x + 2) % NX) * 2 + c

    def other(t):
        return t + 1 - 2 * c

    def multiply(own, t, h):
        rows = pl.ds(h * HALF, HALF)
        block = (x_ref[:, h] if own else xg[t, h]).reshape(HALF, ROWS)
        ks = pl.ds(pl.multiple_of(t * ROWS, ROWS), ROWS)
        acc[rows, WQ:WQ + 320] += lax.dot_general(
            block, wt[:, ks], (((1,), (1,)), ((), ())), preferred_element_type=jnp.float32
        )
        both = jnp.concatenate([dq[ks, :], dk[ks, :]], axis=1)
        acc[rows, DQ:DQ + 256] += jnp.dot(block, both, preferred_element_type=jnp.float32)
        acc[rows, DV:DV + 128] += jnp.dot(block, dv[ks, :], preferred_element_type=jnp.float32)

    def multiply_other(t, h):
        for q in (2 * h, 2 * h + 1):
            arrive_x(other(t), q)
        multiply(False, other(t), h)

    def receive_x(t, q, sem):
        arrive_x(t, q)
        send_x(False, t, q, sibling, sem)

    low = lax.broadcasted_iota(jnp.int32, (QUARTER, 128), 1) < 64
    slot = y % 2

    def head_copies(i, u):
        return [
            remote(msg.at[i, u, pl.ds(0, 256)], kv_ref.at[sp, u], send_a.at[i, u, 0], recv_kv.at[sp, u], partners[i]),
            remote(msg.at[i, u, pl.ds(256, 128)], q_ref.at[slot, u], send_a.at[i, u, 1], recv_q.at[slot, u], partners[i]),
        ]

    def lam_copy(i):
        return remote(lam_ref.at[i], lamo_ref.at[slot], send_lam.at[i], recv_lam.at[slot], partners[i])

    edges = [
        remote(keys.at[pl.ds(WINDOW, WINDOW)], halo_ref.at[1], send_halo.at[1], recv_halo.at[1], before),
        remote(keys.at[pl.ds(ROWS, WINDOW)], halo_ref.at[0], send_halo.at[0], recv_halo.at[0], after),
    ]

    def pack(u):
        first, second = pl.ds(u * HALF, QUARTER), pl.ds(u * HALF + QUARTER, QUARTER)
        k0, k1 = acc[first, DK:DK + 128], acc[second, DK:DK + 128]
        msg[0, u, 0:128] = jnp.where(low, k0, pltpu.roll(k1, 64, 1)).astype(jnp.bfloat16)
        msg[1, u, 0:128] = jnp.where(low, pltpu.roll(k0, 64, 1), k1).astype(jnp.bfloat16)
        for j, part in enumerate((first, second)):
            turned = acc[part, DV:DV + 128].T.astype(jnp.bfloat16)
            asked = (acc[part, DQ:DQ + 128].T * Q_SCALE).astype(jnp.bfloat16)
            for head in range(2):
                msg[head, u, 128 + j * 64:128 + (j + 1) * 64] = turned[head * 64:(head + 1) * 64]
                msg[head, u, 256 + j * 64:256 + (j + 1) * 64] = asked[head * 64:(head + 1) * 64]
        for i in range(2):
            def leave(i=i):
                for copy in head_copies(i, u):
                    copy.start()
            pl.when(away[i])(leave)
            def stay(i=i):
                copies = [
                    pltpu.make_async_copy(msg.at[i, u, pl.ds(0, 256)], kv_ref.at[sp, u], local_sem.at[0]),
                    pltpu.make_async_copy(msg.at[i, u, pl.ds(256, 128)], q_ref.at[slot, u], local_sem.at[1]),
                ]
                for copy in copies:
                    copy.start()
                for copy in copies:
                    copy.wait()
            pl.when(jnp.logical_not(away[i]))(stay)
        for j, part in enumerate((first, second)):
            pair = jnp.where(low, acc[part, 256:384], acc[part, 128:256]).astype(jnp.bfloat16)
            asks = acc[part, 0:256].astype(jnp.bfloat16)
            for g in range(4):
                at = (j * 4 + g) * 2 * SHARE + u * SHARE
                keys[WINDOW + at:WINDOW + at + SHARE] = pair[g * SHARE:(g + 1) * SHARE]
                winq[at:at + SHARE] = asks[g * SHARE:(g + 1) * SHARE]

    def block(zz, s, core):
        return ((zz + NZ) % NZ) * NY + 2 * core + s

    def forward(b, u, device, sem):
        go(remote(kv_ref.at[b, u], kv_ref.at[b, u], sem, recv_kv.at[b, u], device))

    def arrive(b, u):
        remote(kv_ref.at[b, u], kv_ref.at[b, u], send_sib.at[0, 0], recv_kv.at[b, u], sibling).wait_recv()

    def open_ring(u):
        for s in range(2):
            b = block(z, s, c)
            pl.when(away[s])(lambda: arrive(b, u))
            forward(b, u, up, send_ring.at[0, s, u, 0])
            forward(b, u, down, send_ring.at[1, s, u, 0])
            forward(b, u, sibling, send_sib.at[s, u])

    shared = [2, 2]

    def ring(u, d):
        for s in range(2):
            for way, (reach, device, sign) in enumerate(((4 - s, up, -1), (3 + s, down, 1))):
                if d > reach:
                    continue
                b = block(z + sign * d, s, c)
                arrive(b, u)
                if d < reach:
                    forward(b, u, device, send_ring.at[way, s, u, d])
                forward(b, u, sibling, send_sib.at[shared[u], u])
                shared[u] += 1

    def turn(i):
        pair = keys[i * 128:(i + 1) * 128].astype(jnp.float32)
        v_t[:, i * 128:(i + 1) * 128] = pair.T[0:HEAD].astype(jnp.bfloat16)

    def band_edges():
        for copy in edges:
            copy.wait_recv()
        keys[0:WINDOW] = halo_ref[0]
        keys[WINDOW + ROWS:] = halo_ref[1]
        turn(0)
        turn(5)

    def band(i):
        q_t = winq[i * 128:(i + 1) * 128].astype(jnp.float32).T * HEAD ** (-0.5)
        zero = jnp.zeros((HEAD, 128), jnp.float32)
        query = jnp.concatenate(
            [jnp.concatenate([zero, q_t[g * HEAD:(g + 1) * HEAD]], axis=0) for g in range(GROUP)], axis=1
        ).astype(jnp.bfloat16)
        s = jnp.dot(keys[i * 128:i * 128 + 384], query, preferred_element_type=jnp.float32)
        key = lax.broadcasted_iota(jnp.int32, (384, 128), 0)
        ask = lax.broadcasted_iota(jnp.int32, (384, 128), 1)
        start = sp * ROWS + (i - 1) * 128
        allowed = (
            (key - ask >= 0) & (key - ask <= 2 * WINDOW) & (start + key >= 0) & (start + key < live)
        )
        for g in range(GROUP):
            own = jnp.where(allowed, s[:, g * 128:(g + 1) * 128], masked_score)
            top = jnp.maximum(jnp.max(own, axis=0, keepdims=True), sink_ref[g])
            e = jnp.where(allowed, jnp.exp(own - top), 0.0)
            total = jnp.sum(e, axis=0, keepdims=True) + jnp.exp(sink_ref[g] - top)
            o = jnp.dot(v_t[:, i * 128:i * 128 + 384], e.astype(jnp.bfloat16), preferred_element_type=jnp.float32)
            ok = (start + 128 + lax.broadcasted_iota(jnp.int32, (HEAD, 128), 1)) < live
            o = jnp.where(ok, o / total, 0.0)
            both = jnp.concatenate([o, jnp.zeros_like(o)], axis=0).T
            win_ref[i * 128:(i + 1) * 128, g * HEAD:(g + 1) * HEAD] = both[:, 0:HEAD].astype(jnp.bfloat16)

    def nth(i):
        at = i + 4
        d, r = at // 8, at % 8
        sign, core = 2 * (r // 4) - 1, r % 4 // 2
        zz = (z + sign * d + NZ) % NZ
        return zz * NY + 2 * (c + core - 2 * c * core) + r % 2, core == 1

    def set_queries():
        for s in range(2):
            for u in range(2):
                for j in range(2):
                    q = q_ref[s, u, j * 64:(j + 1) * 64, :]
                    for h in range(2):
                        for m in range(2):
                            at = u * TILE + m * ROWS + s * HALF + j * 128
                            qz[h, h * 64 + m * 32:h * 64 + (m + 1) * 32, at:at + 128] = q[m * 32:(m + 1) * 32]

    def set_values(b):
        lane = lax.broadcasted_iota(jnp.int32, (64, 128), 1)
        row = lax.broadcasted_iota(jnp.int32, (16, 128), 0)
        for h in range(2):
            for u in range(2):
                at = h * 256 + u * 128
                ok = b * ROWS + natural(h * 128 + lane, u) < live
                v = kv_ref[b, u, 128 + h * 64:128 + (h + 1) * 64, :].astype(jnp.float32)
                va[0:64, at:at + 128] = jnp.where(ok, v, 0.0).astype(jnp.bfloat16)
                va[64:80, at:at + 128] = jnp.where(ok[:16] & (row == 0), 1.0, 0.0).astype(jnp.bfloat16)

    def set_bias(b):
        row = lax.broadcasted_iota(jnp.int32, (128, 128), 0)
        for h in range(2):
            for u in range(2):
                ok = b * ROWS + natural(h * 128 + row, u) < live
                bias[h, u * 128:(u + 1) * 128] = jnp.where(ok, 0.0, masked_score)

    def score(b, n, h, to):
        k = jnp.concatenate([kv_ref[b, 0, 0:128, :], kv_ref[b, 1, 0:128, :]], axis=0)
        s = jnp.dot(k, qz[h, :, n * TILE:(n + 1) * TILE], preferred_element_type=jnp.float32)
        s = s + jnp.concatenate([bias[h]] * (TILE // 128), axis=1)
        s_buf[to] = s
        t_buf[to] = jnp.max(s.reshape(32, 8, TILE), axis=0)

    def segment(low_i, high_i, ns, fresh):
        units = [(n, h) for n in ns for h in range(2)]
        start = nth(low_i)[0]
        set_bias(start)
        score(start, *units[0], 0)

        def step(i, carry):
            b, _ = nth(i)
            following, foreign = nth(jnp.minimum(i + 1, high_i - 1))
            if fresh:
                @pl.when(jnp.logical_and(foreign, i + 1 < high_i))
                def _():
                    arrive(following, 0)
                    arrive(following, 1)

            set_values(b)
            for j, (n, h) in enumerate(units):
                cols = slice(n * TILE, (n + 1) * TILE)
                s = s_buf[j % 2]
                top = t_buf[j % 2]
                if j + 1 < len(units):
                    score(b, *units[j + 1], 1 - j % 2)
                else:
                    set_bias(following)
                    score(following, *units[0], 1 - j % 2)
                old = m_buf[:, cols]
                new = jnp.maximum(old, jnp.broadcast_to(jnp.max(top, axis=0, keepdims=True), (8, TILE)))
                m_buf[:, cols] = new
                e = jnp.exp2(s.reshape(32, 8, TILE) - new[None]).reshape(256, TILE).astype(jnp.bfloat16)
                held = (att[:, cols].reshape(10, 8, TILE) * jnp.exp2(old - new)[None]).reshape(80, TILE)
                att[:, cols] = held + jnp.dot(
                    va[:, h * 256:(h + 1) * 256], e, preferred_element_type=jnp.float32
                )
            return carry

        lax.fori_loop(low_i, high_i, step, 0)

    def back(n, i):
        return remote(o_buf.at[n, i], rows_t.at[n, slot], send_o.at[n, i], recv_o.at[n, slot], partners[i])

    def finish(n):
        row = gain_ref[...]
        gain = jnp.broadcast_to(jnp.concatenate([row, row], axis=1), (128, 128)).T[0:HEAD]
        lam = lamo_ref[0, 0:1, :]
        lane = lax.broadcasted_iota(jnp.int32, (HEAD, 128), 1)
        for s in range(2):
            for j in range(2):
                maps = []
                for m in range(2):
                    at = n * TILE + m * ROWS + s * HALF + j * 128
                    total = att[64:65, at:at + 128]
                    maps.append(att[0:64, at:at + 128] / jnp.where(total > 0.0, total, 1.0))
                mixed = maps[0] - lam * maps[1]
                normed = mixed * lax.rsqrt(jnp.mean(mixed * mixed, axis=0, keepdims=True) + epsilon) * gain
                ok = (z * NY + 2 * c + s) * ROWS + natural(j * 128 + lane, n) < live
                o_buf[n, s, j * 64:(j + 1) * 64, :] = jnp.where(ok, normed, 0.0).astype(jnp.bfloat16)
        for i in range(2):
            pl.when(away[i])(lambda i=i: back(n, i).start())
            def stay(i=i):
                copy = pltpu.make_async_copy(o_buf.at[n, i], rows_t.at[n, slot], local_sem.at[0])
                copy.start()
                copy.wait()
            pl.when(jnp.logical_not(away[i]))(stay)

    order = (0, 2, 1, 3)

    def owner(side, r):
        return ((x + r) % NX) * 2 + (c if side else 1 - c)

    def partial(n, side, k):
        cols = slice(k * CHUNK, (k + 1) * CHUNK)
        return jnp.dot(lhs_w[n, side], wo[:, cols], preferred_element_type=jnp.float32) + jnp.dot(
            lhs_d[n, side], do[:, cols], preferred_element_type=jnp.float32
        )

    def given(n, k):
        return remote(give.at[n, k], take.at[n, k], send_g.at[n, k], recv_g.at[n, k], sibling)

    def far(n, k):
        return remote(mine.at[n, 2, k], far_in.at[n, k], send_f.at[n, k], recv_f.at[n, k], right if k < 2 else left)

    def near(n, src, k, way):
        return remote(src, fin.at[n, way, k], send_n.at[n, way, k], recv_n.at[n, way, k], left if way else right)

    def merge_give(n):
        for i in range(2):
            def wait(i=i):
                remote(o_buf.at[n, i], rows_t.at[n, i], send_o.at[n, i], recv_o.at[n, i], partners[i]).wait_recv()
            pl.when(away[i])(wait)
        for j in range(2):
            pair = jnp.concatenate(
                [rows_t[n, 0, j * 64:(j + 1) * 64], rows_t[n, 1, j * 64:(j + 1) * 64]], axis=0
            ).astype(jnp.float32)
            diff_rows[j * 128:(j + 1) * 128] = pair.T.astype(jnp.bfloat16)
        for side in range(2):
            for r in range(NX):
                t = owner(side, r)
                to = slice(r * SHARE, (r + 1) * SHARE)
                lhs_w[n, side, to] = win_ref[pl.ds(pl.multiple_of(t * 2 * SHARE + n * SHARE, SHARE), SHARE)]
                lhs_d[n, side, to] = diff_rows[pl.ds(pl.multiple_of(t * SHARE, SHARE), SHARE)]
        for k in order:
            give[n, k] = partial(n, 0, k).astype(jnp.bfloat16)
            go(given(n, k))

    def merge_send(n):
        for k in order:
            own = partial(n, 1, k)
            given(n, k).wait_recv()
            both = (own + take[n, k].astype(jnp.float32)).astype(jnp.bfloat16)
            for r in range(NX):
                mine[n, r, k] = both[r * SHARE:(r + 1) * SHARE]
            go(far(n, k))
        for i in range(2):
            go(near(n, mine.at[n, 1, 2 + i], 2 + i, 0))
            go(near(n, mine.at[n, 3, i], i, 1))

    def merge_join(n):
        for k in order:
            way = 0 if k < 2 else 1
            far(n, k).wait_recv()
            joined[n, k] = (
                mine[n, 3 if way else 1, k].astype(jnp.float32) + far_in[n, k].astype(jnp.float32)
            ).astype(jnp.bfloat16)
            go(near(n, joined.at[n, k], k, way))

    def merge_out(n):
        for k in order:
            near(n, joined.at[n, k], k, 0).wait_recv()
            near(n, joined.at[n, k], k, 1).wait_recv()
            value = (
                mine[n, 0, k].astype(jnp.float32)
                + fin[n, 0, k].astype(jnp.float32)
                + fin[n, 1, k].astype(jnp.float32)
            )
            out_ref[n * SHARE:(n + 1) * SHARE, k * CHUNK:(k + 1) * CHUNK] = value.astype(jnp.bfloat16)

    for q in range(2):
        send_x(True, tp, q, right, send_xr.at[q])
        send_x(True, tp, q, left, send_xl.at[q])
    for q in range(4):
        send_x(True, tp, q, sibling, send_xs.at[q])
    acc[...] = jnp.zeros_like(acc)
    for i in range(2):
        pl.when(away[i])(lambda i=i: lam_copy(i).start())
        def keep(i=i):
            copy = pltpu.make_async_copy(lam_ref.at[i], lamo_ref.at[slot], local_sem.at[2])
            copy.start()
            copy.wait()
        pl.when(jnp.logical_not(away[i]))(keep)
    for load in loads:
        load.wait()
    multiply(True, tp, 0)
    receive_x(t_left, 0, send_xs.at[4])
    send_x(False, t_left, 0, right, send_xr.at[2])
    for q in (2, 3):
        send_x(True, tp, q, right, send_xr.at[q + 1])
    receive_x(t_right, 0, send_xs.at[5])
    multiply(True, tp, 1)
    receive_x(t_right, 1, send_xs.at[6])
    send_x(False, t_right, 1, left, send_xl.at[2])
    for q in (2, 3):
        send_x(True, tp, q, left, send_xl.at[q + 1])
    receive_x(t_left, 1, send_xs.at[7])
    multiply_other(tp, 0)
    multiply_other(tp, 1)
    multiply(False, t_left, 0)
    multiply(False, t_right, 0)
    multiply_other(t_left, 0)
    multiply_other(t_right, 0)
    receive_x(t_far, 0, send_xs.at[8])
    receive_x(t_far, 1, send_xs.at[9])
    multiply(False, t_far, 0)
    multiply_other(t_far, 0)
    pack(0)
    receive_x(t_left, 2, send_xs.at[10])
    send_x(False, t_left, 2, right, send_xr.at[5])
    receive_x(t_right, 2, send_xs.at[11])
    receive_x(t_right, 3, send_xs.at[12])
    send_x(False, t_right, 3, left, send_xl.at[5])
    receive_x(t_left, 3, send_xs.at[13])
    open_ring(0)
    multiply(False, t_left, 1)
    multiply(False, t_right, 1)
    multiply_other(t_left, 1)
    multiply_other(t_right, 1)
    receive_x(t_far, 2, send_xs.at[14])
    receive_x(t_far, 3, send_xs.at[15])
    multiply(False, t_far, 1)
    ring(0, 1)
    multiply_other(t_far, 1)
    pack(1)
    for copy in edges:
        copy.start()
    att[...] = jnp.zeros_like(att)
    va[...] = jnp.zeros_like(va)
    qz[...] = jnp.zeros_like(qz)
    m_buf[...] = jnp.full_like(m_buf, masked_score)
    for i in range(1, 5):
        turn(i)
    band(1)
    band(2)
    open_ring(1)
    for i in range(2):
        def rest(i=i):
            for u in range(2):
                remote(
                    msg.at[0, u, pl.ds(256, 128)], q_ref.at[i, u], send_a.at[0, u, 1], recv_q.at[i, u], sibling
                ).wait_recv()
            remote(lam_ref.at[0], lamo_ref.at[i], send_lam.at[0], recv_lam.at[i], sibling).wait_recv()
        pl.when(away[i])(rest)
    set_queries()
    ring(0, 2)
    segment(0, 4, (0, 1), True)
    ring(0, 3)
    ring(1, 1)
    segment(4, 12, (0, 1), True)
    ring(1, 2)
    ring(0, 4)
    segment(12, 20, (0,), True)
    ring(1, 3)
    segment(20, 28, (0,), True)
    ring(1, 4)
    band_edges()
    band(0)
    band(3)
    segment(28, 32, (0,), True)
    finish(0)
    segment(12, 18, (1,), False)
    merge_give(0)
    segment(18, 20, (1,), False)
    merge_send(0)
    segment(20, 26, (1,), False)
    merge_join(0)
    segment(26, 32, (1,), False)
    finish(1)
    merge_out(0)
    merge_give(1)
    merge_send(1)
    merge_join(1)
    merge_out(1)
    for copy in started + edges:
        copy.wait_send()
    for i in range(2):
        def sent(i=i):
            for u in range(2):
                for copy in head_copies(i, u):
                    copy.wait_send()
                back(u, i).wait_send()
            lam_copy(i).wait_send()
        pl.when(away[i])(sent)


def layer(length, mix_lambda, sink_logit, inputs, gain, weights):
    bf, f32 = jnp.bfloat16, jnp.float32
    depth = weights[3].shape[0]
    width = weights[6].shape[1]
    dma = pltpu.SemaphoreType.DMA
    vmem = pltpu.VMEM
    return pl.pallas_call(
        layer_kernel,
        out_shape=jax.ShapeDtypeStruct((2 * SHARE, width), bf),
        in_specs=[SMEM_SPEC] * 3 + [VMEM_SPEC] * 2 + [HBM_SPEC] * 8,
        out_specs=VMEM_SPEC,
        scratch_shapes=[
            vmem((GROUPS, 2, GROUPS, SHARE, ROWS), bf),
            vmem((320, depth), bf),
            vmem((depth, 128), bf),
            vmem((depth, 128), bf),
            vmem((depth, 128), bf),
            vmem((GROUP * HEAD, width), bf),
            vmem((128, width), bf),
            vmem((ROWS, ACC_COLS), f32),
            vmem((2, 2, 384, 128), bf),
            vmem((2, 8, 128), f32),
            vmem((2, 8, 128), f32),
            vmem((2, WINDOW, 128), bf),
            vmem((ROWS, 256), bf),
            vmem((ROWS + 2 * WINDOW, 128), bf),
            vmem((HEAD, ROWS + 2 * WINDOW), bf),
            vmem((ROWS, GROUP * HEAD), bf),
            vmem((BLOCKS, 2, HALF, 128), bf),
            vmem((2, 2, 128, 128), bf),
            vmem((2, 128, 2 * TILE), bf),
            vmem((80, ROWS), bf),
            vmem((80, 2 * TILE), f32),
            vmem((2, 256, TILE), f32),
            vmem((2, 8, TILE), f32),
            vmem((8, 2 * TILE), f32),
            vmem((2, 256, 128), f32),
            vmem((2, 2, 128, 128), bf),
            vmem((2, 2, 128, 128), bf),
            vmem((HALF, 128), bf),
            vmem((2, 2, 128, GROUP * HEAD), bf),
            vmem((2, 2, 128, 128), bf),
            vmem((2, CHUNKS, 128, CHUNK), bf),
            vmem((2, CHUNKS, 128, CHUNK), bf),
            vmem((2, NX, CHUNKS, SHARE, CHUNK), bf),
            vmem((2, CHUNKS, SHARE, CHUNK), bf),
            vmem((2, CHUNKS, SHARE, CHUNK), bf),
            vmem((2, 2, CHUNKS, SHARE, CHUNK), bf),
            dma((8,)), dma((GROUPS, 4)), dma((6,)), dma((6,)), dma((16,)),
            dma((BLOCKS, 2)), dma((2, 2)), dma((2,)), dma((2,)),
            dma((2, 2, 2)), dma((2,)), dma((2, 2, 2, 4)), dma((16, 2)), dma((2,)), dma((3,)),
            dma((2, 2)), dma((2, 2)), dma((2, CHUNKS)), dma((2, CHUNKS)), dma((2, CHUNKS)), dma((2, CHUNKS)),
            dma((2, 2, CHUNKS)), dma((2, 2, CHUNKS)),
        ],
        compiler_params=pltpu.CompilerParams(
            collective_id=0, has_side_effects=True, vmem_limit_bytes=62 * 1024 * 1024
        ),
        name="layer",
    )(length, mix_lambda, sink_logit, inputs, gain, *weights)


def body(
    inputs, length, win_query, win_key, win_value, sink_logit,
    diff_query, diff_key, diff_value, mix_lambda, head_gain, win_out, diff_out,
):
    weights = (
        win_query.T, win_key.T, win_value.T, diff_query, diff_key, diff_value, win_out, diff_out,
    )
    rows = inputs.reshape(GROUPS, 2, SHARE, inputs.shape[1])
    return layer(length, mix_lambda, sink_logit, rows, head_gain.reshape(1, HEAD), weights)


def solution(mesh):
    placed = (
        P("sp", "tp"), P(), P(None, "tp"), P(None, "tp"), P(None, "tp"), P("tp"), P(None, "tp"),
        P(None, "tp"), P(None, "tp"), P("tp"), P(), P("tp", None), P("tp", None),
    )
    return jax.shard_map(
        body, mesh=mesh, in_specs=placed, out_specs=P(("sp", "tp"), None), check_vma=False
    )
```

profile of v0, /device:TPU:1, one launch (start us, length us, event | category | flops | bytes accessed | tf_op | source)
XLA Modules:
  0.0 113.2 jit_solution(8313965560830031645)
XLA Ops:
  0.7 110.7 %layer.1 = bf16[64,4096]{1,0:T(8,128)(2,1)} custom-call(s32[1]{0:T(128)S(6)} %copy.15.length_ref, f32[2]{0:T(128)} %lam_smem.1, f32[3]{0:T(128)} %sink_ref.1, bf16[8,2,32,512]{3,2,1,0:T(8,128)(2,1)} %bitcast.6, f32[1,64]{1,0:T(1,128)} %bitcast.9, bf16[192,4096]{1,0:T(8,128)(2,1)} %bitcast.5, bf16[64,4096]{1,0:T(8,128)(2,1)} %bitcast.7, ...), custom_call_target="tpu_custom_call" | custom-call | tf_op jit(solution)/shard_map/layer/pallas_call | solution.py:571
  111.3 1.9 %copy.16 = bf16[64,4096]{1,0:T(8,128)(2,1)} copy(bf16[64,4096]{1,0:T(8,128)(2,1)} %layer.1) | data formatting | bytes 1048576
where the time goes:
time: 113 us
  Pallas kernels  111 us (98%)
  local copies, waits for them, and re-layouts  1.87 us (2%)
    pallas_call x1, Pallas kernels, layer(): pl.pallas_call(layer_kernel, out_shape=jax.ShapeDtypeStruct((2 * SHARE, w...  111 us

commit v1 on v0

--- a/solution.py
+++ b/solution.py
@@ -58,9 +58,9 @@
     length_ref, lam_smem, sink_ref, x_ref, gain_ref, wq_hbm, wk_hbm, wv_hbm, dq_hbm, dk_hbm, dv_hbm, wo_hbm, do_hbm,
     out_ref,
     xg, wt, dq, dk, dv, wo, do, acc, msg, lam_ref, lamo_ref, halo_ref, winq, keys, v_t, win_ref,
-    kv_ref, q_ref, qz, va, att, s_buf, t_buf, m_buf, bias,
+    kv_ref, q_ref, qz, va, att, s_buf, t_buf, m_buf, bias, row_at, lane_at,
     o_buf, rows_t, diff_rows, lhs_w, lhs_d, give, take, mine, far_in, joined, fin,
-    w_sem, recv_x, send_xr, send_xl, send_xs,
+    w_sem, recv_x, send_xs,
     recv_kv, recv_q, recv_lam, recv_halo, send_a, send_lam, send_ring, send_sib, send_halo, local_sem,
     recv_o, send_o, send_g, recv_g, send_f, recv_f, send_n, recv_n,
 ):
@@ -102,8 +102,6 @@
     )
     pl.semaphore_wait(pltpu.get_barrier_semaphore(), 7 + sum(a.astype(jnp.int32) for a in away))
 
-    started = []
-
     def remote(src, dst, send_sem, recv_sem, device):
         return pltpu.make_async_remote_copy(
             src_ref=src, dst_ref=dst, send_sem=send_sem, recv_sem=recv_sem,
@@ -112,16 +110,15 @@
 
     def go(copy):
         copy.start()
-        started.append(copy)
-
-    def send_x(own, t, q, device, sem):
+
+    def send_x(own, t, q, device):
         part = pl.ds(q % 2 * 4, 4)
         src = x_ref.at[part, q // 2] if own else xg.at[t, q // 2, part]
-        go(remote(src, xg.at[t, q // 2, part], sem, recv_x.at[t, q], device))
+        go(remote(src, xg.at[t, q // 2, part], send_xs, recv_x.at[t, q], device))
 
     def arrive_x(t, q):
         part = xg.at[t, q // 2, pl.ds(q % 2 * 4, 4)]
-        remote(part, part, send_xr.at[0], recv_x.at[t, q], sibling).wait_recv()
+        remote(part, part, send_xs, recv_x.at[t, q], sibling).wait_recv()
 
     t_left = ((x + NX - 1) % NX) * 2 + c
     t_right = ((x + 1) % NX) * 2 + c
@@ -146,9 +143,9 @@
             arrive_x(other(t), q)
         multiply(False, other(t), h)
 
-    def receive_x(t, q, sem):
+    def receive_x(t, q):
         arrive_x(t, q)
-        send_x(False, t, q, sibling, sem)
+        send_x(False, t, q, sibling)
 
     low = lax.broadcasted_iota(jnp.int32, (QUARTER, 128), 1) < 64
     slot = y % 2
@@ -208,17 +205,15 @@
         go(remote(kv_ref.at[b, u], kv_ref.at[b, u], sem, recv_kv.at[b, u], device))
 
     def arrive(b, u):
-        remote(kv_ref.at[b, u], kv_ref.at[b, u], send_sib.at[0, 0], recv_kv.at[b, u], sibling).wait_recv()
+        remote(kv_ref.at[b, u], kv_ref.at[b, u], send_sib, recv_kv.at[b, u], sibling).wait_recv()
 
     def open_ring(u):
         for s in range(2):
             b = block(z, s, c)
             pl.when(away[s])(lambda: arrive(b, u))
-            forward(b, u, up, send_ring.at[0, s, u, 0])
-            forward(b, u, down, send_ring.at[1, s, u, 0])
-            forward(b, u, sibling, send_sib.at[s, u])
-
-    shared = [2, 2]
+            forward(b, u, up, send_ring)
+            forward(b, u, down, send_ring)
+            forward(b, u, sibling, send_sib)
 
     def ring(u, d):
         for s in range(2):
@@ -228,9 +223,8 @@
                 b = block(z + sign * d, s, c)
                 arrive(b, u)
                 if d < reach:
-                    forward(b, u, device, send_ring.at[way, s, u, d])
-                forward(b, u, sibling, send_sib.at[shared[u], u])
-                shared[u] += 1
+                    forward(b, u, device, send_ring)
+                forward(b, u, sibling, send_sib)
 
     def turn(i):
         pair = keys[i * 128:(i + 1) * 128].astype(jnp.float32)
@@ -285,23 +279,30 @@
                             at = u * TILE + m * ROWS + s * HALF + j * 128
                             qz[h, h * 64 + m * 32:h * 64 + (m + 1) * 32, at:at + 128] = q[m * 32:(m + 1) * 32]
 
+    def set_table():
+        row = lax.broadcasted_iota(jnp.int32, (128, 128), 0)
+        lane = lax.broadcasted_iota(jnp.int32, (8, 128), 1)
+        for h in range(2):
+            for u in range(2):
+                row_at[h, u * 128:(u + 1) * 128] = natural(h * 128 + row, u)
+                lane_at[h, u] = natural(h * 128 + lane, u)
+
     def set_values(b):
-        lane = lax.broadcasted_iota(jnp.int32, (64, 128), 1)
-        row = lax.broadcasted_iota(jnp.int32, (16, 128), 0)
+        top = lax.broadcasted_iota(jnp.int32, (8, 128), 0) == 0
+        zero = jnp.zeros((8, 128), jnp.float32)
         for h in range(2):
             for u in range(2):
                 at = h * 256 + u * 128
-                ok = b * ROWS + natural(h * 128 + lane, u) < live
+                ok = lane_at[h, u] < live - b * ROWS
                 v = kv_ref[b, u, 128 + h * 64:128 + (h + 1) * 64, :].astype(jnp.float32)
-                va[0:64, at:at + 128] = jnp.where(ok, v, 0.0).astype(jnp.bfloat16)
-                va[64:80, at:at + 128] = jnp.where(ok[:16] & (row == 0), 1.0, 0.0).astype(jnp.bfloat16)
+                v = jnp.where(ok[None], v.reshape(8, 8, 128), 0.0).reshape(64, 128)
+                ones = jnp.concatenate([jnp.where(ok & top, 1.0, zero), zero], axis=0)
+                va[0:64, at:at + 128] = v.astype(jnp.bfloat16)
+                va[64:80, at:at + 128] = ones.astype(jnp.bfloat16)
 
     def set_bias(b):
-        row = lax.broadcasted_iota(jnp.int32, (128, 128), 0)
         for h in range(2):
-            for u in range(2):
-                ok = b * ROWS + natural(h * 128 + row, u) < live
-                bias[h, u * 128:(u + 1) * 128] = jnp.where(ok, 0.0, masked_score)
+            bias[h] = jnp.where(row_at[h] < live - b * ROWS, 0.0, masked_score)
 
     def score(b, n, h, to):
         k = jnp.concatenate([kv_ref[b, 0, 0:128, :], kv_ref[b, 1, 0:128, :]], axis=0)
@@ -354,7 +355,6 @@
         row = gain_ref[...]
         gain = jnp.broadcast_to(jnp.concatenate([row, row], axis=1), (128, 128)).T[0:HEAD]
         lam = lamo_ref[0, 0:1, :]
-        lane = lax.broadcasted_iota(jnp.int32, (HEAD, 128), 1)
         for s in range(2):
             for j in range(2):
                 maps = []
@@ -364,7 +364,7 @@
                     maps.append(att[0:64, at:at + 128] / jnp.where(total > 0.0, total, 1.0))
                 mixed = maps[0] - lam * maps[1]
                 normed = mixed * lax.rsqrt(jnp.mean(mixed * mixed, axis=0, keepdims=True) + epsilon) * gain
-                ok = (z * NY + 2 * c + s) * ROWS + natural(j * 128 + lane, n) < live
+                ok = (z * NY + 2 * c + s) * ROWS + lane_at[j, n, 0:1] < live
                 o_buf[n, s, j * 64:(j + 1) * 64, :] = jnp.where(ok, normed, 0.0).astype(jnp.bfloat16)
         for i in range(2):
             pl.when(away[i])(lambda i=i: back(n, i).start())
@@ -386,13 +386,13 @@
         )
 
     def given(n, k):
-        return remote(give.at[n, k], take.at[n, k], send_g.at[n, k], recv_g.at[n, k], sibling)
+        return remote(give.at[n, k], take.at[n, k], send_g, recv_g.at[n, k], sibling)
 
     def far(n, k):
-        return remote(mine.at[n, 2, k], far_in.at[n, k], send_f.at[n, k], recv_f.at[n, k], right if k < 2 else left)
+        return remote(mine.at[n, 2, k], far_in.at[n, k], send_f, recv_f.at[n, k], right if k < 2 else left)
 
     def near(n, src, k, way):
-        return remote(src, fin.at[n, way, k], send_n.at[n, way, k], recv_n.at[n, way, k], left if way else right)
+        return remote(src, fin.at[n, way, k], send_n, recv_n.at[n, way, k], left if way else right)
 
     def merge_give(n):
         for i in range(2):
@@ -447,11 +447,12 @@
             out_ref[n * SHARE:(n + 1) * SHARE, k * CHUNK:(k + 1) * CHUNK] = value.astype(jnp.bfloat16)
 
     for q in range(2):
-        send_x(True, tp, q, right, send_xr.at[q])
-        send_x(True, tp, q, left, send_xl.at[q])
+        send_x(True, tp, q, right)
+        send_x(True, tp, q, left)
     for q in range(4):
-        send_x(True, tp, q, sibling, send_xs.at[q])
+        send_x(True, tp, q, sibling)
     acc[...] = jnp.zeros_like(acc)
+    set_table()
     for i in range(2):
         pl.when(away[i])(lambda i=i: lam_copy(i).start())
         def keep(i=i):
@@ -462,41 +463,41 @@
     for load in loads:
         load.wait()
     multiply(True, tp, 0)
-    receive_x(t_left, 0, send_xs.at[4])
-    send_x(False, t_left, 0, right, send_xr.at[2])
+    receive_x(t_left, 0)
+    send_x(False, t_left, 0, right)
     for q in (2, 3):
-        send_x(True, tp, q, right, send_xr.at[q + 1])
-    receive_x(t_right, 0, send_xs.at[5])
+        send_x(True, tp, q, right)
+    receive_x(t_right, 0)
     multiply(True, tp, 1)
-    receive_x(t_right, 1, send_xs.at[6])
-    send_x(False, t_right, 1, left, send_xl.at[2])
+    receive_x(t_right, 1)
+    send_x(False, t_right, 1, left)
     for q in (2, 3):
-        send_x(True, tp, q, left, send_xl.at[q + 1])
-    receive_x(t_left, 1, send_xs.at[7])
+        send_x(True, tp, q, left)
+    receive_x(t_left, 1)
     multiply_other(tp, 0)
     multiply_other(tp, 1)
     multiply(False, t_left, 0)
     multiply(False, t_right, 0)
     multiply_other(t_left, 0)
     multiply_other(t_right, 0)
-    receive_x(t_far, 0, send_xs.at[8])
-    receive_x(t_far, 1, send_xs.at[9])
+    receive_x(t_far, 0)
+    receive_x(t_far, 1)
     multiply(False, t_far, 0)
     multiply_other(t_far, 0)
     pack(0)
-    receive_x(t_left, 2, send_xs.at[10])
-    send_x(False, t_left, 2, right, send_xr.at[5])
-    receive_x(t_right, 2, send_xs.at[11])
-    receive_x(t_right, 3, send_xs.at[12])
-    send_x(False, t_right, 3, left, send_xl.at[5])
-    receive_x(t_left, 3, send_xs.at[13])
+    receive_x(t_left, 2)
+    send_x(False, t_left, 2, right)
+    receive_x(t_right, 2)
+    receive_x(t_right, 3)
+    send_x(False, t_right, 3, left)
+    receive_x(t_left, 3)
     open_ring(0)
     multiply(False, t_left, 1)
     multiply(False, t_right, 1)
     multiply_other(t_left, 1)
     multiply_other(t_right, 1)
-    receive_x(t_far, 2, send_xs.at[14])
-    receive_x(t_far, 3, send_xs.at[15])
+    receive_x(t_far, 2)
+    receive_x(t_far, 3)
     multiply(False, t_far, 1)
     ring(0, 1)
     multiply_other(t_far, 1)
@@ -550,7 +551,16 @@
     merge_send(1)
     merge_join(1)
     merge_out(1)
-    for copy in started + edges:
+    for ref, sem in (
+        (xg.at[pl.ds(0, 7)], send_xs),
+        (kv_ref.at[pl.ds(0, 14)], send_ring),
+        (kv_ref.at[pl.ds(0, 16)], send_sib),
+        (give, send_g),
+        (joined, send_f),
+        (fin, send_n),
+    ):
+        remote(ref, ref, sem, recv_x.at[0, 0], sibling).wait_send()
+    for copy in edges:
         copy.wait_send()
     for i in range(2):
         def sent(i=i):
@@ -599,6 +609,8 @@
             vmem((2, 8, TILE), f32),
             vmem((8, 2 * TILE), f32),
             vmem((2, 256, 128), f32),
+            vmem((2, 256, 128), jnp.int32),
+            vmem((2, 2, 8, 128), jnp.int32),
             vmem((2, 2, 128, 128), bf),
             vmem((2, 2, 128, 128), bf),
             vmem((HALF, 128), bf),
@@ -610,11 +622,11 @@
             vmem((2, CHUNKS, SHARE, CHUNK), bf),
             vmem((2, CHUNKS, SHARE, CHUNK), bf),
             vmem((2, 2, CHUNKS, SHARE, CHUNK), bf),
-            dma((8,)), dma((GROUPS, 4)), dma((6,)), dma((6,)), dma((16,)),
+            dma((8,)), dma((GROUPS, 4)), dma,
             dma((BLOCKS, 2)), dma((2, 2)), dma((2,)), dma((2,)),
-            dma((2, 2, 2)), dma((2,)), dma((2, 2, 2, 4)), dma((16, 2)), dma((2,)), dma((3,)),
-            dma((2, 2)), dma((2, 2)), dma((2, CHUNKS)), dma((2, CHUNKS)), dma((2, CHUNKS)), dma((2, CHUNKS)),
-            dma((2, 2, CHUNKS)), dma((2, 2, CHUNKS)),
+            dma((2, 2, 2)), dma((2,)), dma, dma, dma((2,)), dma((3,)),
+            dma((2, 2)), dma((2, 2)), dma, dma((2, CHUNKS)), dma, dma((2, CHUNKS)),
+            dma, dma((2, 2, CHUNKS)),
         ],
         compiler_params=pltpu.CompilerParams(
             collective_id=0, has_side_effects=True, vmem_limit_bytes=62 * 1024 * 1024

time: 113 us -> 112 us (level)
  Pallas kernels: 111 us -> 109 us
    pallas_call x1, Pallas kernels: 111 us -> 109 us  [layer(): pl.pallas_call(layer_kernel, out_shape=jax.ShapeDtypeStruct((2 * SHARE, w...]
where the time goes in v1:
time: 112 us
  Pallas kernels  109 us (97%)
  local copies, waits for them, and re-layouts  1.87 us (2%)
    pallas_call x1, Pallas kernels, layer(): pl.pallas_call(layer_kernel, out_shape=jax.ShapeDtypeStruct((2 * SHARE, w...  109 us

profile of v1, /device:TPU:1, one launch (start us, length us, event | category | flops | bytes accessed | tf_op | source)
XLA Modules:
  0.0 112.0 jit_solution(3941624616598127777)
XLA Ops:
  0.7 109.4 %layer.1 = bf16[64,4096]{1,0:T(8,128)(2,1)} custom-call(s32[1]{0:T(128)S(6)} %copy.15.length_ref, f32[2]{0:T(128)} %lam_smem.1, f32[3]{0:T(128)} %sink_ref.1, bf16[8,2,32,512]{3,2,1,0:T(8,128)(2,1)} %bitcast.6, f32[1,64]{1,0:T(1,128)} %bitcast.9, bf16[192,4096]{1,0:T(8,128)(2,1)} %bitcast.5, bf16[64,4096]{1,0:T(8,128)(2,1)} %bitcast.7, ...), custom_call_target="tpu_custom_call" | custom-call | tf_op jit(solution)/shard_map/layer/pallas_call | solution.py:581
  110.1 1.9 %copy.16 = bf16[64,4096]{1,0:T(8,128)(2,1)} copy(bf16[64,4096]{1,0:T(8,128)(2,1)} %layer.1) | data formatting | bytes 1048576

commit v2 on v1

--- a/solution.py
+++ b/solution.py
@@ -170,7 +170,9 @@
         msg[0, u, 0:128] = jnp.where(low, k0, pltpu.roll(k1, 64, 1)).astype(jnp.bfloat16)
         msg[1, u, 0:128] = jnp.where(low, pltpu.roll(k0, 64, 1), k1).astype(jnp.bfloat16)
         for j, part in enumerate((first, second)):
-            turned = acc[part, DV:DV + 128].T.astype(jnp.bfloat16)
+            turned = jnp.where(
+                lane_at[j, u, 0:1] < live - sp * ROWS, acc[part, DV:DV + 128].T, 0.0
+            ).astype(jnp.bfloat16)
             asked = (acc[part, DQ:DQ + 128].T * Q_SCALE).astype(jnp.bfloat16)
             for head in range(2):
                 msg[head, u, 128 + j * 64:128 + (j + 1) * 64] = turned[head * 64:(head + 1) * 64]
@@ -287,18 +289,15 @@
                 row_at[h, u * 128:(u + 1) * 128] = natural(h * 128 + row, u)
                 lane_at[h, u] = natural(h * 128 + lane, u)
 
-    def set_values(b):
+    def set_ones(b, g):
         top = lax.broadcasted_iota(jnp.int32, (8, 128), 0) == 0
         zero = jnp.zeros((8, 128), jnp.float32)
         for h in range(2):
             for u in range(2):
                 at = h * 256 + u * 128
                 ok = lane_at[h, u] < live - b * ROWS
-                v = kv_ref[b, u, 128 + h * 64:128 + (h + 1) * 64, :].astype(jnp.float32)
-                v = jnp.where(ok[None], v.reshape(8, 8, 128), 0.0).reshape(64, 128)
                 ones = jnp.concatenate([jnp.where(ok & top, 1.0, zero), zero], axis=0)
-                va[0:64, at:at + 128] = v.astype(jnp.bfloat16)
-                va[64:80, at:at + 128] = ones.astype(jnp.bfloat16)
+                va[g, :, at:at + 128] = ones.astype(jnp.bfloat16)
 
     def set_bias(b):
         for h in range(2):
@@ -312,41 +311,51 @@
         t_buf[to] = jnp.max(s.reshape(32, 8, TILE), axis=0)
 
     def segment(low_i, high_i, ns, fresh):
-        units = [(n, h) for n in ns for h in range(2)]
+        group = 2 // len(ns)
+        units = [(g, n, h) for g in range(group) for n in ns for h in range(2)]
         start = nth(low_i)[0]
         set_bias(start)
-        score(start, *units[0], 0)
-
-        def step(i, carry):
-            b, _ = nth(i)
-            following, foreign = nth(jnp.minimum(i + 1, high_i - 1))
-            if fresh:
-                @pl.when(jnp.logical_and(foreign, i + 1 < high_i))
-                def _():
-                    arrive(following, 0)
-                    arrive(following, 1)
-
-            set_values(b)
-            for j, (n, h) in enumerate(units):
+        score(start, *units[0][1:], 0)
+
+        def step(trip, carry):
+            i = low_i + trip * group
+            blocks = [nth(i)[0]]
+            for g in range(1, group + 1):
+                following, foreign = nth(jnp.minimum(i + g, high_i - 1))
+                blocks.append(following)
+                if fresh:
+                    def wait(following=following):
+                        arrive(following, 0)
+                        arrive(following, 1)
+                    pl.when(jnp.logical_and(foreign, i + g < high_i))(wait)
+
+            for j, (g, n, h) in enumerate(units):
+                b = blocks[g]
                 cols = slice(n * TILE, (n + 1) * TILE)
+                if j == 0 or units[j - 1][0] != g:
+                    set_ones(b, g)
                 s = s_buf[j % 2]
                 top = t_buf[j % 2]
-                if j + 1 < len(units):
-                    score(b, *units[j + 1], 1 - j % 2)
-                else:
-                    set_bias(following)
-                    score(following, *units[0], 1 - j % 2)
+                g_next, n_next, h_next = units[j + 1] if j + 1 < len(units) else (group,) + units[0][1:]
+                if g_next != g:
+                    set_bias(blocks[g_next])
+                score(blocks[g_next], n_next, h_next, 1 - j % 2)
                 old = m_buf[:, cols]
                 new = jnp.maximum(old, jnp.broadcast_to(jnp.max(top, axis=0, keepdims=True), (8, TILE)))
                 m_buf[:, cols] = new
                 e = jnp.exp2(s.reshape(32, 8, TILE) - new[None]).reshape(256, TILE).astype(jnp.bfloat16)
                 held = (att[:, cols].reshape(10, 8, TILE) * jnp.exp2(old - new)[None]).reshape(80, TILE)
-                att[:, cols] = held + jnp.dot(
-                    va[:, h * 256:(h + 1) * 256], e, preferred_element_type=jnp.float32
+                value = jnp.concatenate(
+                    [
+                        jnp.concatenate([kv_ref[b, u, 128 + h * 64:192 + h * 64, :] for u in range(2)], axis=1),
+                        va[g, :, h * 256:(h + 1) * 256],
+                    ],
+                    axis=0,
                 )
+                att[:, cols] = held + jnp.dot(value, e, preferred_element_type=jnp.float32)
             return carry
 
-        lax.fori_loop(low_i, high_i, step, 0)
+        lax.fori_loop(0, (high_i - low_i) // group, step, 0)
 
     def back(n, i):
         return remote(o_buf.at[n, i], rows_t.at[n, slot], send_o.at[n, i], recv_o.at[n, slot], partners[i])
@@ -448,7 +457,7 @@
 
     for q in range(2):
         send_x(True, tp, q, right)
-        send_x(True, tp, q, left)
+        send_x(True, tp, 1 - q, left)
     for q in range(4):
         send_x(True, tp, q, sibling)
     acc[...] = jnp.zeros_like(acc)
@@ -467,13 +476,13 @@
     send_x(False, t_left, 0, right)
     for q in (2, 3):
         send_x(True, tp, q, right)
-    receive_x(t_right, 0)
-    multiply(True, tp, 1)
     receive_x(t_right, 1)
     send_x(False, t_right, 1, left)
-    for q in (2, 3):
+    for q in (3, 2):
         send_x(True, tp, q, left)
+    multiply(True, tp, 1)
     receive_x(t_left, 1)
+    receive_x(t_right, 0)
     multiply_other(tp, 0)
     multiply_other(tp, 1)
     multiply(False, t_left, 0)
@@ -487,9 +496,9 @@
     pack(0)
     receive_x(t_left, 2)
     send_x(False, t_left, 2, right)
-    receive_x(t_right, 2)
     receive_x(t_right, 3)
     send_x(False, t_right, 3, left)
+    receive_x(t_right, 2)
     receive_x(t_left, 3)
     open_ring(0)
     multiply(False, t_left, 1)
@@ -505,7 +514,6 @@
     for copy in edges:
         copy.start()
     att[...] = jnp.zeros_like(att)
-    va[...] = jnp.zeros_like(va)
     qz[...] = jnp.zeros_like(qz)
     m_buf[...] = jnp.full_like(m_buf, masked_score)
     for i in range(1, 5):
@@ -603,7 +611,7 @@
             vmem((BLOCKS, 2, HALF, 128), bf),
             vmem((2, 2, 128, 128), bf),
             vmem((2, 128, 2 * TILE), bf),
-            vmem((80, ROWS), bf),
+            vmem((2, 16, ROWS), bf),
             vmem((80, 2 * TILE), f32),
             vmem((2, 256, TILE), f32),
             vmem((2, 8, TILE), f32),

time: 112 us -> 109 us (0.973)
  Pallas kernels: 109 us -> 106 us
    pallas_call x1, Pallas kernels: 109 us -> 106 us  [layer(): pl.pallas_call(layer_kernel, out_shape=jax.ShapeDtypeStruct((2 * SHARE, w...]
where the time goes in v2:
time: 109 us
  Pallas kernels  106 us (97%)
  local copies, waits for them, and re-layouts  1.87 us (2%)
    pallas_call x1, Pallas kernels, layer(): pl.pallas_call(layer_kernel, out_shape=jax.ShapeDtypeStruct((2 * SHARE, w...  106 us

profile of v2, /device:TPU:1, one launch (start us, length us, event | category | flops | bytes accessed | tf_op | source)
XLA Modules:
  0.0 108.8 jit_solution(13143493012582138063)
XLA Ops:
  0.7 106.2 %layer.1 = bf16[64,4096]{1,0:T(8,128)(2,1)} custom-call(s32[1]{0:T(128)S(6)} %copy.15.length_ref, f32[2]{0:T(128)} %lam_smem.1, f32[3]{0:T(128)} %sink_ref.1, bf16[8,2,32,512]{3,2,1,0:T(8,128)(2,1)} %bitcast.6, f32[1,64]{1,0:T(1,128)} %bitcast.9, bf16[192,4096]{1,0:T(8,128)(2,1)} %bitcast.5, bf16[64,4096]{1,0:T(8,128)(2,1)} %bitcast.7, ...), custom_call_target="tpu_custom_call" | custom-call | tf_op jit(solution)/shard_map/layer/pallas_call | solution.py:589
  106.9 1.9 %copy.16 = bf16[64,4096]{1,0:T(8,128)(2,1)} copy(bf16[64,4096]{1,0:T(8,128)(2,1)} %layer.1) | data formatting | bytes 1048576

commit v3 on v2

--- a/solution.py
+++ b/solution.py
@@ -311,7 +311,7 @@
         t_buf[to] = jnp.max(s.reshape(32, 8, TILE), axis=0)
 
     def segment(low_i, high_i, ns, fresh):
-        group = 2 // len(ns)
+        group = 2
         units = [(g, n, h) for g in range(group) for n in ns for h in range(2)]
         start = nth(low_i)[0]
         set_bias(start)
@@ -548,15 +548,14 @@
     finish(0)
     segment(12, 18, (1,), False)
     merge_give(0)
-    segment(18, 20, (1,), False)
+    segment(18, 24, (1,), False)
     merge_send(0)
-    segment(20, 26, (1,), False)
+    segment(24, 32, (1,), False)
+    finish(1)
     merge_join(0)
-    segment(26, 32, (1,), False)
-    finish(1)
-    merge_out(0)
     merge_give(1)
     merge_send(1)
+    merge_out(0)
     merge_join(1)
     merge_out(1)
     for ref, sem in (

time: 109 us -> 109 us (level)
  no operation moved by 1% of the time
where the time goes in v3:
time: 109 us
  Pallas kernels  107 us (98%)
  local copies, waits for them, and re-layouts  1.87 us (2%)
    pallas_call x1, Pallas kernels, layer(): pl.pallas_call(layer_kernel, out_shape=jax.ShapeDtypeStruct((2 * SHARE, w...  107 us

profile of v3, /device:TPU:1, one launch (start us, length us, event | category | flops | bytes accessed | tf_op | source)
XLA Modules:
  0.0 109.1 jit_solution(15660380550357340473)
XLA Ops:
  0.7 106.6 %layer.1 = bf16[64,4096]{1,0:T(8,128)(2,1)} custom-call(s32[1]{0:T(128)S(6)} %copy.15.length_ref, f32[2]{0:T(128)} %lam_smem.1, f32[3]{0:T(128)} %sink_ref.1, bf16[8,2,32,512]{3,2,1,0:T(8,128)(2,1)} %bitcast.6, f32[1,64]{1,0:T(1,128)} %bitcast.9, bf16[192,4096]{1,0:T(8,128)(2,1)} %bitcast.5, bf16[64,4096]{1,0:T(8,128)(2,1)} %bitcast.7, ...), custom_call_target="tpu_custom_call" | custom-call | tf_op jit(solution)/shard_map/layer/pallas_call | solution.py:588
  107.2 1.9 %copy.16 = bf16[64,4096]{1,0:T(8,128)(2,1)} copy(bf16[64,4096]{1,0:T(8,128)(2,1)} %layer.1) | data formatting | bytes 1048576
